TPU v7x, 32 devices: a whole 2x2x4 slice. The times are simulated.
32 devices in a mesh: sp: 8 (over z, y), tp: 4 (over x, core).
Axes of the slice: x: 2, y: 2, z: 4, core: 2. Of those that a mesh axis runs over, the one named last changes fastest.
Arguments:
- tokens: bfloat16 [6144, 2048], P('sp', 'tp'), may hold values from -18 to 18
- proj_weight: bfloat16 [2048, 1024], P(None, 'tp'), may hold values from -0.125 to 0.125
- gate_weight: bfloat16 [2048, 1024], P(None, 'tp'), may hold values from -0.125 to 0.125
- conv_weight: float32 [4, 1024], replicated, may hold values from -3 to 3
- recur_weight: bfloat16 [16, 64, 64], replicated, may hold values from -0.75 to 0.75
- input_weight: bfloat16 [16, 64, 64], replicated, may hold values from -0.75 to 0.75
- decay_param: float32 [1024], replicated, as said below
- out_grad: bfloat16 [6144, 1024], P('sp', 'tp'), may hold values from -6 to 6
Outputs:
- d_proj: bfloat16 [6144, 1024], P('sp', 'tp')
- d_gate: bfloat16 [6144, 1024], P('sp', 'tp')
- d_weight: float32 [2048, 1024], P('sp', 'tp')
Inputs may be any that keep to these rules, and one draw needn't show every extreme that they name: `decay_param`: every channel's decay parameter is at least 4; there is no fixed upper bound.
All inputs are finite; a program needn't handle non-finite values.
Results may differ from a plain program's by a relative error of at most 0.01.
Values may be sent and summed in bfloat16 or wider, within the bound.
A program may use at most 64 MiB of HBM per device.

v0:
```python
import jax
import jax.numpy as jnp
from jax import lax
from jax.sharding import PartitionSpec as P

BLOCK = 64
rate_scale = 8.0
scale_floor = 0.0001


def from_behind(value, axis, steps):
    count = lax.axis_size(axis)
    first, last = (max(0, -steps), min(count, count - steps))
    return lax.ppermute(value, axis, [(source, source + steps) for source in range(first, last)])


def combine(earlier, later):
    return (earlier[0] * later[0], later[0] * earlier[1] + later[1])


def block_map(values, weights, block_count):
    row_count = values.shape[0]
    shaped = values.reshape(row_count, block_count, BLOCK)
    result = jnp.einsum("tgi,gij->tgj", shaped, weights, preferred_element_type=jnp.float32)
    return result.reshape(row_count, block_count * BLOCK)


def block_back(values, weights, block_count):
    row_count = values.shape[0]
    shaped = values.reshape(row_count, block_count, BLOCK)
    result = jnp.einsum("tgj,gij->tgi", shaped, weights, preferred_element_type=jnp.float32)
    return result.reshape(row_count, block_count * BLOCK)


def per_device(
    tokens, proj_weight, gate_weight, conv_weight, recur_weight, input_weight, decay_param, out_grad
):
    tp_index = lax.axis_index("tp")
    row_count = tokens.shape[0]
    chan_width = proj_weight.shape[1]
    block_count = chan_width // BLOCK
    gathered = lax.all_gather(tokens, "tp", axis=1, tiled=True)
    projected = jnp.dot(gathered, proj_weight, preferred_element_type=jnp.float32).astype(
        jnp.bfloat16
    )
    gate_in = jnp.dot(gathered, gate_weight, preferred_element_type=jnp.float32).astype(
        jnp.bfloat16
    )
    conv_taps = lax.dynamic_slice_in_dim(conv_weight, tp_index * chan_width, chan_width, 1)
    decay_slice = lax.dynamic_slice_in_dim(decay_param, tp_index * chan_width, chan_width, 0)
    w_recur = lax.dynamic_slice_in_dim(recur_weight, tp_index * block_count, block_count, 0)
    w_input = lax.dynamic_slice_in_dim(input_weight, tp_index * block_count, block_count, 0)
    prior_rows = from_behind(projected[row_count - 3 :], "sp", 1)
    padded = jnp.concatenate([prior_rows, projected], axis=0).astype(jnp.float32)
    total = conv_taps[0] * padded[3 : 3 + row_count]
    for offset in range(1, 4):
        total = total + conv_taps[offset] * padded[3 - offset : 3 - offset + row_count]
    conv_out = total.astype(jnp.bfloat16)
    conv_float = conv_out.astype(jnp.float32)
    recur_open = jax.nn.sigmoid(block_map(conv_out, w_recur, block_count))
    input_open = jax.nn.sigmoid(block_map(conv_out, w_input, block_count))
    log_slope = rate_scale * jax.nn.log_sigmoid(decay_slice)
    log_decay = log_slope * recur_open
    decay_rate = jnp.exp(log_decay)
    input_scale = jnp.sqrt(scale_floor - jnp.expm1(2.0 * log_decay))
    gated_input = input_open * conv_float
    drive = input_scale * gated_input
    cum_decay, local_states = lax.associative_scan(combine, (decay_rate, drive), axis=0)
    gelu_gate, gelu_back = jax.vjp(jax.nn.gelu, gate_in.astype(jnp.float32))
    cotangent = out_grad.astype(jnp.float32)
    drive_grad = cotangent * gelu_gate
    shifted = jnp.concatenate([decay_rate[1:], jnp.ones((1, chan_width), jnp.float32)], axis=0)
    cum_after, local_grad = lax.associative_scan(
        combine, (shifted, drive_grad), reverse=True, axis=0
    )
    span_decay = cum_decay[-1]
    span_state = local_states[-1]
    span_grad = decay_rate[0] * local_grad[0]
    all_decay, all_state, all_grad = (
        lax.all_gather(span_decay[None], "sp", axis=0, tiled=True),
        lax.all_gather(span_state[None], "sp", axis=0, tiled=True),
        lax.all_gather(span_grad[None], "sp", axis=0, tiled=True),
    )
    sp_index = lax.axis_index("sp")
    sp_count = lax.axis_size("sp")
    _, fwd_state = lax.associative_scan(combine, (all_decay, all_state), axis=0)
    _, rev_grad = lax.associative_scan(combine, (all_decay, all_grad), reverse=True, axis=0)
    before = lax.dynamic_index_in_dim(fwd_state, jnp.maximum(sp_index - 1, 0), 0, False)
    after = lax.dynamic_index_in_dim(rev_grad, jnp.minimum(sp_index + 1, sp_count - 1), 0, False)
    carry_state = jnp.where(sp_index > 0, before, 0.0)
    carry_grad = jnp.where(sp_index < sp_count - 1, after, 0.0)
    states = local_states + cum_decay * carry_state
    previous = jnp.concatenate([carry_state[None], states[:-1]], axis=0)
    d_gate = gelu_back(cotangent * states)[0].astype(jnp.bfloat16)
    state_grad = local_grad + cum_after * carry_grad
    d_log_decay = state_grad * (
        decay_rate * previous - gated_input * decay_rate * decay_rate / input_scale
    )
    d_recur_pre = (d_log_decay * log_slope * recur_open * (1.0 - recur_open)).astype(jnp.bfloat16)
    d_input_pre = (state_grad * input_scale * conv_float * input_open * (1.0 - input_open)).astype(
        jnp.bfloat16
    )
    d_conv = state_grad * input_scale * input_open
    d_conv = d_conv + block_back(d_recur_pre, w_recur, block_count)
    d_conv = d_conv + block_back(d_input_pre, w_input, block_count)
    next_rows = from_behind(d_conv[:3], "sp", -1)
    extended = jnp.concatenate([d_conv, next_rows], axis=0)
    grad_sum = conv_taps[0] * extended[0:row_count]
    for offset in range(1, 4):
        grad_sum = grad_sum + conv_taps[offset] * extended[offset : offset + row_count]
    d_proj = grad_sum.astype(jnp.bfloat16)
    d_weight = lax.psum_scatter(
        lax.dot_general(
            gathered, d_proj, (((0,), (0,)), ((), ())), preferred_element_type=jnp.float32
        ),
        "sp",
        scatter_dimension=0,
        tiled=True,
    )
    return (d_proj, d_gate, d_weight)


def solution(mesh):
    in_specs = (P("sp", "tp"), P(None, "tp"), P(None, "tp"), P(), P(), P(), P(), P("sp", "tp"))
    out_specs = (P("sp", "tp"), P("sp", "tp"), P("sp", "tp"))
    return jax.shard_map(
        per_device, mesh=mesh, in_specs=in_specs, out_specs=out_specs, check_vma=False
    )
```

profile of v0, /device:TPU:0, one launch (start us, length us, event | category | flops | bytes accessed | tf_op | source)
XLA Modules:
  0.0 441.6 jit_solution(7558327511127030171)
XLA Ops:
  8.9 31.9 %all-gather.5.cloned.1.call-done = bf16[768,2048]{1,0:T(8,128)(2,1)} async-done(((bf16[768,512]{1,0:T(8,128)(2,1)}), bf16[768,2048]{1,0:T(8,128)(2,1)}) %all-gather.5.cloned.1.call-update) | async-done | bytes 3145744 | tf_op jit(solution)/shard_map/all_gather | solution.py:42
  40.8 3.1 convolution_convert_fusion
  44.0 3.4 collective-permute-start
  53.6 2.0 fusion.38
  57.1 3.2 slice.964
  60.3 3.2 slice.924
  63.5 3.2 slice.923
  71.6 2.2 multiply_add_fusion.2
  75.1 1.7 slice.962
  81.4 1.7 slice.894
  86.4 1.9 multiply_add_fusion.4
  124.2 2.0 pad.329
  126.2 2.0 pad.305
  136.1 2.1 pad.330
  138.2 2.1 pad.331
  140.3 2.1 pad.307
  145.5 1.8 fusion.44
  151.0 2.3 pad.333
  153.2 2.3 pad.309
  155.5 1.7 add.563
  157.3 1.7 add.601
  159.0 2.1 fusion.42
  161.8 2.5 pad.310
  165.9 2.5 pad.334
  168.3 2.5 pad.335
  170.8 2.5 pad.311
  173.3 2.0 add.564
  175.3 1.9 add.603
  177.2 2.5 fusion.40
  180.5 2.9 pad.336
  183.4 3.0 pad.337
  187.1 21.3 %all-gather.2 = f32[8,1,256]{2,1,0:T(1,128)S(1)} all-gather(f32[1,1,256]{2,1,0:T(1,128)S(1)} %add_bitcast_fusion), channel_id=1, replica_groups=mesh['sp'=8,'tp'=4] {'sp'}, dimensions={0}, use_global_device_ids=true | all-gather | bytes 9216 | tf_op jit(solution)/shard_map/all_gather | solution.py:81
  208.4 1.8 pad_maximum_fusion.2
  210.2 2.9 pad.312
  213.2 2.9 pad.313
  216.7 16.5 %all-gather.1 = f32[8,1,256]{2,1,0:T(1,128)S(1)} all-gather(f32[1,1,256]{2,1,0:T(1,128)S(1)} %add_bitcast_fusion.1), channel_id=1, replica_groups=mesh['sp'=8,'tp'=4] {'sp'}, dimensions={0}, use_global_device_ids=true | all-gather | bytes 9216 | tf_op jit(solution)/shard_map/all_gather | solution.py:80
  233.7 5.5 %fusion.12 = (bf16[768,256]{1,0:T(8,128)(2,1)}, f32[768,256]{1,0:T(8,128)}, f32[768,256]{1,0:T(8,128)S(1)}) fusion(bf16[768,256]{1,0:T(8,128)(2,1)} %param.15, f32[256]{0:T(256)S(1)} %bitcast.89, f32[768,256]{1,0:T(8,128)} %pad.312, f32[768,256]{1,0:T(8,128)} %pad.313, f32[768,256]{1,0:T(8,128)} %pad.336, f32[768,256]{1,0:T(8,128)} %pad.337, ...), kind=kOutput, calls=%fused_computation.29 | convolution fusion | flops 811204608 | bytes 9700352 | tf_op jit(solution)/shard_map/dot_general | solution.py:46
  240.1 3.2 slice.834
  243.3 3.1 slice.768
  246.4 3.1 slice.766
  254.1 3.9 slice.767
  258.0 3.8 slice.769
  261.8 3.8 slice.772
  265.6 3.8 slice.765
  278.7 2.1 slice.835
  280.8 4.0 slice.763
  292.5 2.5 pad.293
  294.9 2.5 pad.275
  297.4 1.8 add.545
  299.2 1.8 add.555
  301.0 2.3 add_multiply_fusion.2
  305.2 3.0 pad.277
  310.1 18.3 %all-gather = f32[8,1,256]{2,1,0:T(1,128)S(1)} all-gather(f32[1,1,256]{2,1,0:T(1,128)S(1)} %fusion.85), channel_id=1, replica_groups=mesh['sp'=8,'tp'=4] {'sp'}, dimensions={0}, use_global_device_ids=true | all-gather | bytes 9216 | tf_op jit(solution)/shard_map/all_gather | solution.py:82
  328.9 1.8 concatenate.151
  331.4 2.9 pad.294
  334.3 3.0 pad.295
  337.2 2.4 add.556
  339.6 6.8 %rev.14 = f32[768,256]{1,0:T(8,128)} reverse(f32[768,256]{1,0:T(8,128)} %add.556), dimensions={0} | reverse | bytes 1572864 | tf_op jit(solution)/shard_map/rev | solution.py:73
  346.5 3.7 fusion.9
  352.8 1.9 copy.49
  360.0 4.2 collective-permute-done.1
  364.6 2.3 convolution_bitcast_fusion
  366.9 66.0 %reduce-scatter.2.cloned.1.call-done = f32[256,256]{0,1:T(8,128)} async-done(((f32[2048,256]{0,1:T(8,128)}), f32[256,256]{0,1:T(8,128)}) %reduce-scatter.2.cloned.1.call-update) | async-done | bytes 262160 | tf_op jit(solution)/shard_map/reduce_scatter | solution.py:112
  432.9 1.8 copy.57
  (407 shorter events, 113.8 us)
Async XLA Ops:
  7.2 226.6 %copy-start = (bf16[2048,256]{1,0:T(8,128)(2,1)S(1)}, bf16[2048,256]{1,0:T(8,128)(2,1)}, u32[]{:S(2)}) copy-start(bf16[2048,256]{1,0:T(8,128)(2,1)} %param.10) | copy-start | bytes 3145732
  7.2 33.6 %all-gather.5.cloned.1.call-start = ((), (), s32[]{:S(2)}) async-start(), calls=%async_computation.1 | async-start | bytes 3932160 | tf_op jit(solution)/shard_map/all_gather | solution.py:42
  7.9 425.0 %reduce-scatter.2.cloned.1.call-start = ((), (), s32[]{:S(2)}) async-start(), calls=%async_computation.2 | async-start | bytes 2359296 | tf_op jit(solution)/shard_map/reduce_scatter | solution.py:112
  8.9 44.7 %copy-start.14 = (f32[1,256]{1,0:T(1,128)}, f32[1,256]{1,0:T(1,128)S(1)}, u32[]{:S(2)}) copy-start(f32[1,256]{1,0:T(1,128)S(1)} %get-tuple-element.76) | copy-start | bytes 3076
  8.9 44.7 %copy-start.16 = (f32[1,256]{1,0:T(1,128)}, f32[1,256]{1,0:T(1,128)S(1)}, u32[]{:S(2)}) copy-start(f32[1,256]{1,0:T(1,128)S(1)} %get-tuple-element.77) | copy-start | bytes 3076
  8.9 44.7 %copy-start.18 = (f32[1,256]{1,0:T(1,128)}, f32[1,256]{1,0:T(1,128)S(1)}, u32[]{:S(2)}) copy-start(f32[1,256]{1,0:T(1,128)S(1)} %get-tuple-element.78) | copy-start | bytes 3076
  8.9 44.6 %copy-start.20 = (f32[1,256]{1,0:T(1,128)}, f32[1,256]{1,0:T(1,128)S(1)}, u32[]{:S(2)}) copy-start(f32[1,256]{1,0:T(1,128)S(1)} %get-tuple-element.79) | copy-start | bytes 3076
  44.0 4.7 %collective-permute-start = (bf16[3,256]{1,0:T(4,128)(2,1)S(1)}, bf16[3,256]{1,0:T(4,128)(2,1)S(1)}, u32[]{:S(2)}, u32[]{:S(2)}) collective-permute-start(bf16[3,256]{1,0:T(4,128)(2,1)S(1)} %slice.991), channel_id=1, source_target_pairs={{0,4},{4,8},{8,12},{12,16},{16,20},{20,24},{24,28},{1,5},{5,9},{9,... | collective-permute-start | bytes 4616 | tf_op jit(solution)/shard_map/ppermute | solution.py:14
  48.1 5.4 %copy-start.22 = (f32[256]{0:T(256)}, f32[256]{0:T(256)S(1)}, u32[]{:S(2)}) copy-start(f32[256]{0:T(256)S(1)} %fusion.82) | copy-start | bytes 3076
  49.3 1.4 copy-start.13
  55.6 0.9 copy-start.3
  73.8 0.7 copy-start.6
  88.4 0.7 copy-start.10
  101.4 0.6 copy-start.12
  120.2 27.1 %copy-start.29 = (f32[1,256]{1,0:T(1,128)S(1)}, f32[1,256]{1,0:T(1,128)}, u32[]{:S(2)}) copy-start(f32[1,256]{1,0:T(1,128)} %slice.1054) | copy-start | bytes 3076
  120.2 28.5 %copy-start.28 = (f32[1,256]{1,0:T(1,128)S(1)}, f32[1,256]{1,0:T(1,128)}, u32[]{:S(2)}) copy-start(f32[1,256]{1,0:T(1,128)} %slice.1094) | copy-start | bytes 3076
  134.7 26.4 %copy-start.27 = (f32[1,256]{1,0:T(1,128)S(1)}, f32[1,256]{1,0:T(1,128)}, u32[]{:S(2)}) copy-start(f32[1,256]{1,0:T(1,128)} %slice.1053) | copy-start | bytes 3076
  143.9 20.3 %copy-start.26 = (f32[1,256]{1,0:T(1,128)S(1)}, f32[1,256]{1,0:T(1,128)}, u32[]{:S(2)}) copy-start(f32[1,256]{1,0:T(1,128)} %slice.1093) | copy-start | bytes 3076
  170.8 8.8 %copy-start.25 = (f32[1,256]{1,0:T(1,128)S(1)}, f32[1,256]{1,0:T(1,128)}, u32[]{:S(2)}) copy-start(f32[1,256]{1,0:T(1,128)} %slice.1092) | copy-start | bytes 3076
  177.2 31.2 %copy-start.24 = (f32[1,256]{1,0:T(1,128)S(1)}, f32[1,256]{1,0:T(1,128)}, u32[]{:S(2)}) copy-start(f32[1,256]{1,0:T(1,128)} %slice.1049) | copy-start | bytes 3076
  233.7 5.5 %copy-start.30 = (f32[1,256]{1,0:T(1,128)}, f32[1,256]{1,0:T(1,128)S(1)}, u32[]{:S(2)}) copy-start(f32[1,256]{1,0:T(1,128)S(1)} %broadcast_select_fusion) | copy-start | bytes 3076
  239.2 0.9 copy-start.7
  273.3 5.4 %copy-start.8 = (f32[383,256]{1,0:T(8,128)S(1)}, f32[383,256]{1,0:T(8,128)}, u32[]{:S(2)}) copy-start(f32[383,256]{1,0:T(8,128)} %slice.834) | copy-start | bytes 1176580
  285.2 4.5 %copy-start.11 = (f32[191,256]{1,0:T(8,128)S(1)}, f32[191,256]{1,0:T(8,128)}, u32[]{:S(2)}) copy-start(f32[191,256]{1,0:T(8,128)} %slice.773) | copy-start | bytes 586756
  331.3 15.1 %copy-start.2 = (f32[768,256]{1,0:T(8,128)S(1)}, f32[768,256]{1,0:T(8,128)}, u32[]{:S(2)}) copy-start(f32[768,256]{1,0:T(8,128)} %copy.43) | copy-start | bytes 2359300
  331.3 15.1 %copy-start.15 = (f32[1,256]{1,0:T(1,128)S(1)}, f32[1,256]{1,0:T(1,128)}, u32[]{:S(2)}) copy-start(f32[1,256]{1,0:T(1,128)} %copy-done.14) | copy-start | bytes 3076
  331.3 15.1 %copy-start.17 = (f32[1,256]{1,0:T(1,128)S(1)}, f32[1,256]{1,0:T(1,128)}, u32[]{:S(2)}) copy-start(f32[1,256]{1,0:T(1,128)} %copy-done.16) | copy-start | bytes 3076
  331.3 15.1 %copy-start.19 = (f32[1,256]{1,0:T(1,128)S(1)}, f32[1,256]{1,0:T(1,128)}, u32[]{:S(2)}) copy-start(f32[1,256]{1,0:T(1,128)} %copy-done.18) | copy-start | bytes 3076
  331.3 15.1 %copy-start.21 = (f32[1,256]{1,0:T(1,128)S(1)}, f32[1,256]{1,0:T(1,128)}, u32[]{:S(2)}) copy-start(f32[1,256]{1,0:T(1,128)} %copy-done.20) | copy-start | bytes 3076
  331.3 15.1 %copy-start.23 = (f32[256]{0:T(256)S(1)}, f32[256]{0:T(256)}, u32[]{:S(2)}) copy-start(f32[256]{0:T(256)} %copy-done.22) | copy-start | bytes 3076
  331.4 15.1 %copy-start.31 = (f32[1,256]{1,0:T(1,128)S(1)}, f32[1,256]{1,0:T(1,128)}, u32[]{:S(2)}) copy-start(f32[1,256]{1,0:T(1,128)} %copy-done.30) | copy-start | bytes 3076
  351.3 5.8 %copy-start.5 = (f32[768,256]{1,0:T(8,128)S(1)}, f32[768,256]{1,0:T(8,128)}, u32[]{:S(2)}) copy-start(f32[768,256]{1,0:T(8,128)} %get-tuple-element.17) | copy-start | bytes 2359300
  357.1 7.4 %copy-start.4 = (bf16[768,2048]{1,0:T(8,128)(2,1)S(1)}, bf16[768,2048]{1,0:T(8,128)(2,1)}, u32[]{:S(2)}) copy-start(bf16[768,2048]{1,0:T(8,128)(2,1)} %all-gather.5.cloned.1.call-done) | copy-start | bytes 9437188
  358.7 5.5 %collective-permute-start.1 = (f32[3,256]{1,0:T(4,128)S(1)}, f32[3,256]{1,0:T(4,128)S(1)}, u32[]{:S(2)}, u32[]{:S(2)}) collective-permute-start(f32[3,256]{1,0:T(4,128)S(1)} %slice.1134), channel_id=1, source_target_pairs={{4,0},{8,4},{12,8},{16,12},{20,16},{24,20},{28,24},{5,1},{9,5},{13... | collective-permute-start | bytes 9224 | tf_op jit(solution)/shard_map/ppermute | solution.py:14
  364.2 70.5 %copy-start.1 = (bf16[2048,256]{1,0:T(8,128)(2,1)S(1)}, bf16[2048,256]{1,0:T(8,128)(2,1)}, u32[]{:S(2)}) copy-start(bf16[2048,256]{1,0:T(8,128)(2,1)} %param.10) | copy-start | bytes 3145732
  364.6 2.3 copy-start.9
Sparse Core Ops, SparseCore 0:
  9.6 31.2 all-gather.4
  367.0 65.8 reduce-scatter.1
where the time goes:
time: 447 us; the launch traced here: 442 us
  local copies, waits for them, and re-layouts  172 us (38%)
  waiting for transfers between devices  103 us (23%)
  other arithmetic  73.5 us (16%)
  blocking collectives  56.1 us (13%)
  matrix products  16.1 us (4%)
  between operations  15.5 us (3%)
  starting transfers between devices  4.75 us (1%)
    reduce_scatter x1, waiting for transfers between devices, per_device(): lax.psum_scatter(lax.dot_general(gathered, d_proj, (((0,), (0,)), ((), ()...  66 us
    slice x63, local copies, waits for them, and re-layouts, per_device(): lax.associative_scan(combine, (decay_rate, drive), axis=0)  51 us
    slice x69, local copies, waits for them, and re-layouts, per_device(): lax.associative_scan(combine, (shifted, drive_grad), reverse=True, axis=0)  41.5 us
    pad x34, local copies, waits for them, and re-layouts, per_device(): lax.associative_scan(combine, (decay_rate, drive), axis=0)  40.1 us
    all_gather x1, waiting for transfers between devices, per_device(): gathered = lax.all_gather(tokens, 'tp', axis=1, tiled=True)  31.9 us
    all_gather x1, blocking collectives, per_device(): lax.all_gather(span_state[None], 'sp', axis=0, tiled=True)  21.3 us
    all_gather x1, blocking collectives, per_device(): lax.all_gather(span_grad[None], 'sp', axis=0, tiled=True)  18.3 us
    add x22, other arithmetic, combine(): return (earlier[0] * later[0], later[0] * earlier[1] + later[1])  17.5 us
  transfers between devices with their start and end apart: 4, of which 4 were waited for; matrix products, arithmetic and copies ran while one was open for 0% of the time, Pallas kernels for 0%

commit v1 on v0

--- a/solution.py
+++ b/solution.py
@@ -39,7 +39,14 @@
     row_count = tokens.shape[0]
     chan_width = proj_weight.shape[1]
     block_count = chan_width // BLOCK
-    gathered = lax.all_gather(tokens, "tp", axis=1, tiled=True)
+    n_dev = lax.axis_size("tp")
+    route = [(i, (i + 1) % n_dev) for i in range(n_dev)]
+    parts = [tokens]
+    for far in range(1, n_dev):
+        parts = [lax.ppermute(parts[0], "tp", route), *parts]
+    full = jnp.concatenate(parts, axis=1)
+    offset_2 = (lax.axis_index("tp") + 1) * parts[-1].shape[1]
+    gathered = jnp.roll(full, offset_2, axis=1)
     projected = jnp.dot(gathered, proj_weight, preferred_element_type=jnp.float32).astype(
         jnp.bfloat16
     )

time: 447 us -> 460 us (1.029)
  local copies, waits for them, and re-layouts: 172 us -> 182 us
    ppermute x0 -> x3, waiting for transfers between devices: none -> 33.7 us  [per_device(): parts = [lax.ppermute(parts[0], 'tp', route), *parts]]
    all_gather x1 -> x0, waiting for transfers between devices: 31.9 us -> none  [per_device(): gathered = lax.all_gather(tokens, 'tp', axis=1, tiled=True)]
    unnamed x68 -> x66, local copies, waits for them, and re-layouts: 5.82 us -> 10.7 us
    rev x2, local copies, waits for them, and re-layouts: 7.14 us -> 12 us  [per_device(): lax.associative_scan(combine, (shifted, drive_grad), reverse=True, axis=0)]
  transfers between devices with their start and end apart: 4 -> 6, of which waited for: 4 -> 6; matrix products, arithmetic and copies ran while one was open for 0% -> 0% of each run, Pallas kernels for 0% -> 0%
where the time goes in v1:
time: 460 us; the launch traced here: 454 us
  local copies, waits for them, and re-layouts  182 us (40%)
  waiting for transfers between devices  105 us (23%)
  other arithmetic  73.4 us (16%)
  blocking collectives  56.3 us (12%)
  matrix products  15.9 us (3%)
  between operations  15.5 us (3%)
  starting transfers between devices  6.15 us (1%)
    reduce_scatter x1, waiting for transfers between devices, per_device(): lax.psum_scatter(lax.dot_general(gathered, d_proj, (((0,), (0,)), ((), ()...  66 us
    slice x63, local copies, waits for them, and re-layouts, per_device(): lax.associative_scan(combine, (decay_rate, drive), axis=0)  50.5 us
    slice x69, local copies, waits for them, and re-layouts, per_device(): lax.associative_scan(combine, (shifted, drive_grad), reverse=True, axis=0)  40.9 us
    pad x34, local copies, waits for them, and re-layouts, per_device(): lax.associative_scan(combine, (decay_rate, drive), axis=0)  40.2 us
    ppermute x3, waiting for transfers between devices, per_device(): parts = [lax.ppermute(parts[0], 'tp', route), *parts]  33.7 us
    all_gather x1, blocking collectives, per_device(): lax.all_gather(span_state[None], 'sp', axis=0, tiled=True)  21.6 us
    all_gather x1, blocking collectives, per_device(): lax.all_gather(span_grad[None], 'sp', axis=0, tiled=True)  18.3 us
    add x22, other arithmetic, combine(): return (earlier[0] * later[0], later[0] * earlier[1] + later[1])  17.5 us
  transfers between devices with their start and end apart: 6, of which 6 were waited for; matrix products, arithmetic and copies ran while one was open for 0% of the time, Pallas kernels for 0%

profile of v1, /device:TPU:0, one launch (start us, length us, event | category | flops | bytes accessed | tf_op | source)
XLA Modules:
  0.0 454.0 jit_solution(11432817123174443376)
XLA Ops:
  7.8 11.8 %collective-permute-done = bf16[768,512]{1,0:T(8,128)(2,1)S(1)} collective-permute-done((bf16[768,512]{1,0:T(8,128)(2,1)}, bf16[768,512]{1,0:T(8,128)(2,1)S(1)}, u32[]{:S(2)}, u32[]{:S(2)}) %collective-permute-start) | collective-permute-done | bytes 786464 | tf_op jit(solution)/shard_map/ppermute | solution.py:46
  19.6 11.4 %collective-permute-done.1 = bf16[768,512]{1,0:T(8,128)(2,1)S(1)} collective-permute-done((bf16[768,512]{1,0:T(8,128)(2,1)S(1)}, bf16[768,512]{1,0:T(8,128)(2,1)S(1)}, u32[]{:S(2)}, u32[]{:S(2)}) %collective-permute-start.1) | collective-permute-done | bytes 786464 | tf_op jit(solution)/shard_map/ppermute | solution.py:46
  32.0 10.6 %collective-permute-done.2 = bf16[768,512]{1,0:T(8,128)(2,1)} collective-permute-done((bf16[768,512]{1,0:T(8,128)(2,1)S(1)}, bf16[768,512]{1,0:T(8,128)(2,1)}, u32[]{:S(2)}, u32[]{:S(2)}) %collective-permute-start.2) | collective-permute-done | bytes 786464 | tf_op jit(solution)/shard_map/ppermute | solution.py:46
  46.7 2.6 copy-done.12
  50.4 4.2 collective-permute-start.3
  60.8 2.0 fusion.50
  64.4 3.2 slice.964
  67.5 3.2 slice.924
  70.7 3.2 slice.923
  78.8 2.2 multiply_add_fusion.2
  93.6 1.9 multiply_add_fusion.4
  131.0 2.0 pad.329
  133.0 2.0 pad.305
  142.8 2.1 pad.330
  144.9 2.1 pad.331
  146.9 2.1 pad.307
  152.2 1.8 fusion.56
  158.3 2.3 pad.333
  160.5 2.3 pad.309
  166.2 2.1 fusion.54
  169.0 2.5 pad.310
  173.1 2.5 pad.334
  175.7 2.5 pad.335
  178.2 2.5 pad.311
  180.7 1.9 add.580
  182.6 1.9 add.619
  184.5 2.5 fusion.52
  187.8 2.9 pad.336
  190.7 3.0 pad.337
  194.4 21.6 %all-gather.2 = f32[8,1,256]{2,1,0:T(1,128)S(1)} all-gather(f32[1,1,256]{2,1,0:T(1,128)S(1)} %add_bitcast_fusion), channel_id=1, replica_groups=mesh['sp'=8,'tp'=4] {'sp'}, dimensions={0}, use_global_device_ids=true | all-gather | bytes 9216 | tf_op jit(solution)/shard_map/all_gather | solution.py:88
  216.0 1.8 pad_maximum_fusion.2
  217.8 2.9 pad.312
  220.7 2.9 pad.313
  224.3 16.5 %all-gather.1 = f32[8,1,256]{2,1,0:T(1,128)S(1)} all-gather(f32[1,1,256]{2,1,0:T(1,128)S(1)} %add_bitcast_fusion.1), channel_id=1, replica_groups=mesh['sp'=8,'tp'=4] {'sp'}, dimensions={0}, use_global_device_ids=true | all-gather | bytes 9216 | tf_op jit(solution)/shard_map/all_gather | solution.py:87
  241.3 5.5 %fusion.24 = (bf16[768,256]{1,0:T(8,128)(2,1)}, f32[768,256]{1,0:T(8,128)}, f32[768,256]{1,0:T(8,128)S(1)}) fusion(bf16[768,256]{1,0:T(8,128)(2,1)} %param.15, f32[256]{0:T(256)S(1)} %bitcast.84, f32[768,256]{1,0:T(8,128)} %pad.312, f32[768,256]{1,0:T(8,128)} %pad.313, f32[768,256]{1,0:T(8,128)} %pad.336, f32[768,256]{1,0:T(8,128)} %pad.337, ...), kind=kOutput, calls=%fused_computation.34 | convolution fusion | flops 811204608 | bytes 9700356 | tf_op jit(solution)/shard_map/dot_general | solution.py:53
  247.7 3.2 slice.834
  250.9 3.1 slice.768
  254.0 3.1 slice.766
  261.7 3.9 slice.767
  265.5 3.9 slice.769
  269.4 3.9 slice.772
  273.3 3.8 slice.765
  283.7 4.0 slice.835
  287.7 3.9 slice.763
  298.4 2.5 pad.293
  300.9 2.6 pad.275
  303.4 1.8 add.561
  305.2 1.8 add.571
  307.0 2.3 add_multiply_fusion.2
  309.3 1.9 pad.276
  311.2 3.0 pad.277
  314.9 2.4 add.563
  317.3 18.3 %all-gather = f32[8,1,256]{2,1,0:T(1,128)S(1)} all-gather(f32[1,1,256]{2,1,0:T(1,128)S(1)} %fusion.100), channel_id=1, replica_groups=mesh['sp'=8,'tp'=4] {'sp'}, dimensions={0}, use_global_device_ids=true | all-gather | bytes 9216 | tf_op jit(solution)/shard_map/all_gather | solution.py:89
  336.1 1.8 concatenate.158
  337.8 5.1 %rev.6 = f32[768,256]{1,0:T(8,128)S(1)} reverse(f32[768,256]{1,0:T(8,128)} %add.563), dimensions={0} | reverse | bytes 1572864 | tf_op jit(solution)/shard_map/rev | solution.py:80
  343.3 2.9 pad.294
  346.1 3.0 pad.295
  349.1 2.4 add.572
  351.5 6.8 %rev.14 = f32[768,256]{1,0:T(8,128)} reverse(f32[768,256]{1,0:T(8,128)} %add.572), dimensions={0} | reverse | bytes 1572864 | tf_op jit(solution)/shard_map/rev | solution.py:80
  358.4 3.7 fusion.21
  369.0 1.7 add_add_fusion
  372.0 4.2 collective-permute-done.4
  376.6 4.5 fusion
  381.1 66.0 %reduce-scatter.2.cloned.1.call-done = f32[256,256]{1,0:T(8,128)} async-done(((f32[2048,256]{1,0:T(8,128)}), f32[256,256]{1,0:T(8,128)}) %reduce-scatter.2.cloned.1.call-update) | async-done | bytes 262160 | tf_op jit(solution)/shard_map/reduce_scatter | solution.py:119
  (409 shorter events, 119.0 us)
Async XLA Ops:
  7.2 234.1 %copy-start = (bf16[2048,256]{1,0:T(8,128)(2,1)S(1)}, bf16[2048,256]{1,0:T(8,128)(2,1)}, u32[]{:S(2)}) copy-start(bf16[2048,256]{1,0:T(8,128)(2,1)} %param.10) | copy-start | bytes 3145732
  7.2 39.4 %copy-start.4 = (bf16[768,512]{1,0:T(8,128)(2,1)S(1)}, bf16[768,512]{1,0:T(8,128)(2,1)}, u32[]{:S(2)}) copy-start(bf16[768,512]{1,0:T(8,128)(2,1)} %param.8) | copy-start | bytes 2359300
  7.2 439.9 %reduce-scatter.2.cloned.1.call-start = ((), (), s32[]{:S(2)}) async-start(), calls=%async_computation.1 | async-start | bytes 2359296 | tf_op jit(solution)/shard_map/reduce_scatter | solution.py:119
  7.2 12.3 %collective-permute-start = (bf16[768,512]{1,0:T(8,128)(2,1)}, bf16[768,512]{1,0:T(8,128)(2,1)S(1)}, u32[]{:S(2)}, u32[]{:S(2)}) collective-permute-start(bf16[768,512]{1,0:T(8,128)(2,1)} %param.8), channel_id=1, source_target_pairs={{0,1},{1,2},{2,3},{3,0},{4,5},{5,6},{6,7},{7,4},{8,9},{9,10},{10,1... | collective-permute-start | bytes 2359304 | tf_op jit(solution)/shard_map/ppermute | solution.py:46
  19.6 11.4 %collective-permute-start.1 = (bf16[768,512]{1,0:T(8,128)(2,1)S(1)}, bf16[768,512]{1,0:T(8,128)(2,1)S(1)}, u32[]{:S(2)}, u32[]{:S(2)}) collective-permute-start(bf16[768,512]{1,0:T(8,128)(2,1)S(1)} %collective-permute-done), channel_id=1, source_target_pairs={{0,1},{1,2},{2,3},{3,0},{4,5},{5,6},{6,7},{7,4},{8,9},{9,10},{10,1... | collective-permute-start | bytes 2359304 | tf_op jit(solution)/shard_map/ppermute | solution.py:46
  31.0 11.5 %collective-permute-start.2 = (bf16[768,512]{1,0:T(8,128)(2,1)S(1)}, bf16[768,512]{1,0:T(8,128)(2,1)}, u32[]{:S(2)}, u32[]{:S(2)}) collective-permute-start(bf16[768,512]{1,0:T(8,128)(2,1)S(1)} %collective-permute-done.1), channel_id=1, source_target_pairs={{0,1},{1,2},{2,3},{3,0},{4,5},{5,6},{6,7},{7,4},{8,9},{9,10},{10,1... | collective-permute-start | bytes 2359304 | tf_op jit(solution)/shard_map/ppermute | solution.py:46
  31.9 28.9 %copy-start.13 = (f32[1,256]{1,0:T(1,128)}, f32[1,256]{1,0:T(1,128)S(1)}, u32[]{:S(2)}) copy-start(f32[1,256]{1,0:T(1,128)S(1)} %get-tuple-element.67) | copy-start | bytes 3076
  31.9 28.9 %copy-start.15 = (f32[1,256]{1,0:T(1,128)}, f32[1,256]{1,0:T(1,128)S(1)}, u32[]{:S(2)}) copy-start(f32[1,256]{1,0:T(1,128)S(1)} %get-tuple-element.68) | copy-start | bytes 3076
  31.9 28.9 %copy-start.17 = (f32[1,256]{1,0:T(1,128)}, f32[1,256]{1,0:T(1,128)S(1)}, u32[]{:S(2)}) copy-start(f32[1,256]{1,0:T(1,128)S(1)} %get-tuple-element.69) | copy-start | bytes 3076
  31.9 28.9 %copy-start.19 = (f32[1,256]{1,0:T(1,128)}, f32[1,256]{1,0:T(1,128)S(1)}, u32[]{:S(2)}) copy-start(f32[1,256]{1,0:T(1,128)S(1)} %get-tuple-element.70) | copy-start | bytes 3076
  31.9 17.4 %copy-start.27 = (bf16[2048,256]{1,0:T(8,128)(2,1)S(1)}, bf16[2048,256]{1,0:T(8,128)(2,1)}, u32[]{:S(2)}) copy-start(bf16[2048,256]{1,0:T(8,128)(2,1)} %param.9) | copy-start | bytes 3145732
  46.7 2.6 copy-start.12
  50.4 5.5 %collective-permute-start.3 = (bf16[3,256]{1,0:T(4,128)(2,1)S(1)}, bf16[3,256]{1,0:T(4,128)(2,1)S(1)}, u32[]{:S(2)}, u32[]{:S(2)}) collective-permute-start(bf16[3,256]{1,0:T(4,128)(2,1)S(1)} %slice.991), channel_id=1, source_target_pairs={{0,4},{4,8},{8,12},{12,16},{16,20},{20,24},{24,28},{1,5},{5,9},{9,... | collective-permute-start | bytes 4616 | tf_op jit(solution)/shard_map/ppermute | solution.py:14
  55.4 5.4 %copy-start.21 = (f32[256]{0:T(256)}, f32[256]{0:T(256)S(1)}, u32[]{:S(2)}) copy-start(f32[256]{0:T(256)S(1)} %fusion.97) | copy-start | bytes 3076
  56.5 1.4 copy-start.10
  62.9 0.9 copy-start.3
  81.0 0.7 copy-start.6
  95.5 0.7 copy-start.8
  108.5 0.6 copy-start.9
  127.0 41.3 %copy-start.26 = (f32[1,256]{1,0:T(1,128)S(1)}, f32[1,256]{1,0:T(1,128)}, u32[]{:S(2)}) copy-start(f32[1,256]{1,0:T(1,128)} %slice.1053) | copy-start | bytes 3076
  127.0 44.5 %copy-start.25 = (f32[1,256]{1,0:T(1,128)S(1)}, f32[1,256]{1,0:T(1,128)}, u32[]{:S(2)}) copy-start(f32[1,256]{1,0:T(1,128)} %slice.1093) | copy-start | bytes 3076
  156.0 31.1 %copy-start.24 = (f32[1,256]{1,0:T(1,128)S(1)}, f32[1,256]{1,0:T(1,128)}, u32[]{:S(2)}) copy-start(f32[1,256]{1,0:T(1,128)} %slice.1092) | copy-start | bytes 3076
  168.3 47.7 %copy-start.23 = (f32[1,256]{1,0:T(1,128)S(1)}, f32[1,256]{1,0:T(1,128)}, u32[]{:S(2)}) copy-start(f32[1,256]{1,0:T(1,128)} %slice.1049) | copy-start | bytes 3076
  246.8 0.9 copy-start.7
  311.2 47.1 %copy-start.2 = (f32[768,256]{1,0:T(8,128)S(1)}, f32[768,256]{1,0:T(8,128)}, u32[]{:S(2)}) copy-start(f32[768,256]{1,0:T(8,128)} %copy.41) | copy-start | bytes 2359300
  311.2 47.1 %copy-start.14 = (f32[1,256]{1,0:T(1,128)S(1)}, f32[1,256]{1,0:T(1,128)}, u32[]{:S(2)}) copy-start(f32[1,256]{1,0:T(1,128)} %copy-done.13) | copy-start | bytes 3076
  311.2 47.1 %copy-start.16 = (f32[1,256]{1,0:T(1,128)S(1)}, f32[1,256]{1,0:T(1,128)}, u32[]{:S(2)}) copy-start(f32[1,256]{1,0:T(1,128)} %copy-done.15) | copy-start | bytes 3076
  311.2 47.1 %copy-start.18 = (f32[1,256]{1,0:T(1,128)S(1)}, f32[1,256]{1,0:T(1,128)}, u32[]{:S(2)}) copy-start(f32[1,256]{1,0:T(1,128)} %copy-done.17) | copy-start | bytes 3076
  311.2 47.1 %copy-start.20 = (f32[1,256]{1,0:T(1,128)S(1)}, f32[1,256]{1,0:T(1,128)}, u32[]{:S(2)}) copy-start(f32[1,256]{1,0:T(1,128)} %copy-done.19) | copy-start | bytes 3076
  311.2 47.1 %copy-start.22 = (f32[256]{0:T(256)S(1)}, f32[256]{0:T(256)}, u32[]{:S(2)}) copy-start(f32[256]{0:T(256)} %copy-done.21) | copy-start | bytes 3076
  362.1 6.9 %copy-start.5 = (f32[768,256]{1,0:T(8,128)S(1)}, f32[768,256]{1,0:T(8,128)}, u32[]{:S(2)}) copy-start(f32[768,256]{1,0:T(8,128)} %get-tuple-element.8) | copy-start | bytes 2359300
  369.0 78.2 %copy-start.1 = (bf16[2048,256]{1,0:T(8,128)(2,1)S(1)}, bf16[2048,256]{1,0:T(8,128)(2,1)}, u32[]{:S(2)}) copy-start(bf16[2048,256]{1,0:T(8,128)(2,1)} %param.10) | copy-start | bytes 3145732
  370.7 5.5 %collective-permute-start.4 = (f32[3,256]{1,0:T(4,128)S(1)}, f32[3,256]{1,0:T(4,128)S(1)}, u32[]{:S(2)}, u32[]{:S(2)}) collective-permute-start(f32[3,256]{1,0:T(4,128)S(1)} %slice.1134), channel_id=1, source_target_pairs={{4,0},{8,4},{12,8},{16,12},{20,16},{24,20},{28,24},{5,1},{9,5},{13... | collective-permute-start | bytes 9224 | tf_op jit(solution)/shard_map/ppermute | solution.py:14
  376.6 70.5 %copy-start.11 = (bf16[768,256]{1,0:T(8,128)(2,1)}, bf16[768,256]{1,0:T(8,128)(2,1)S(1)}, u32[]{:S(2)}) copy-start(bf16[768,256]{1,0:T(8,128)(2,1)S(1)} %fusion.29) | copy-start | bytes 1179652
Sparse Core Ops, SparseCore 0:
  381.2 65.8 reduce-scatter.1
